TPU v7x, 128 devices: a whole 4x4x4 slice. The times are simulated.
128 devices in a mesh: ep: 16 (over z, x), tp: 8 (over y, core).
Axes of the slice: x: 4, y: 4, z: 4, core: 2. Of those that a mesh axis runs over, the one named last changes fastest.
Arguments:
- mixer_rows: bfloat16 [4096, 4096], P('ep'), may hold values from -8 to 8, as said below
- mixer_gain: float32 [4096], replicated, may hold values from 0.1 to 1.9
- gate_proj: bfloat16 [4096, 4096], P(None, 'tp'), may hold values from -0.09375 to 0.09375
- input_proj: bfloat16 [4096, 4096], P(None, 'tp'), may hold values from -0.09375 to 0.09375
- conv_taps: float32 [4, 4096], P(None, 'tp'), may hold values from -2 to 2
- input_gates: bfloat16 [16, 256, 256], P('tp'), may hold values from -0.375 to 0.375
- decay_gates: bfloat16 [16, 256, 256], P('tp'), may hold values from -0.375 to 0.375
- decay_offset: float32 [4096], P('tp'), may hold values from 4.8 to 13, as said below
- out_proj: bfloat16 [4096, 4096], P('tp'), may hold values from -0.09375 to 0.09375
- mixer_scale: float32 [4096], replicated, may hold values from 0.1 to 1.9
- expert_rows: bfloat16 [4096, 4096], P('ep'), may hold values from -6 to 6
- expert_gain: float32 [4096], replicated, may hold values from 0.1 to 1.9
- route_ids: int32 [4096, 2], P('ep'), may hold values from 0 to 15, all different within a row; in each aligned block of 256 rows (0 to 255, 256 to 511, ...) at most 48 rows name the same one
- route_weights: float32 [4096, 2], P('ep'), may hold values from 0.5 to 2
- expert_gate: bfloat16 [16, 4096, 1024], P('ep', None, 'tp'), may hold values from -0.09375 to 0.09375
- expert_up: bfloat16 [16, 4096, 1024], P('ep', None, 'tp'), may hold values from -0.09375 to 0.09375
- expert_down: bfloat16 [16, 1024, 4096], P('ep', 'tp'), may hold values from -0.1875 to 0.1875
- shared_gate: bfloat16 [4096, 1024], P(None, 'tp'), may hold values from -0.09375 to 0.09375
- shared_up: bfloat16 [4096, 1024], P(None, 'tp'), may hold values from -0.09375 to 0.09375
- shared_down: bfloat16 [1024, 4096], P('tp'), may hold values from -0.1875 to 0.1875
- expert_scale: float32 [4096], replicated, may hold values from 0.1 to 1.9
Outputs:
- mixer_out: bfloat16 [4096, 4096], P(('ep', 'tp'))
- expert_out: bfloat16 [4096, 4096], P(('ep', 'tp'))
Inputs may be any that keep to these rules, and one draw needn't show every extreme that they name: `mixer_rows`: order one, with a common direction whose weight drifts slowly along the sequence. `decay_offset`: the even channels forget within some 30 to 200 tokens; the odd channels keep 5 to 90 percent of their state over the whole sequence of 4096 tokens. `route_ids`: each row names 2 different experts; within the rows of one index of ep (aligned blocks of 256 rows) no expert is named by more than 48 rows, and in some blocks one is named by exactly 48.
All inputs are finite; a program needn't handle non-finite values.
Results may differ from a plain program's by a relative error of at most 0.0033.
The roundings to bfloat16 on the way count: a program that leaves them out, or rounds other values in their place, can miss the bound.
Values may be sent and summed in bfloat16 or wider, within the bound.
A program may use at most 192 MiB of HBM per device.

v0:
```python
import jax
import jax.numpy as jnp
from jax import lax
from jax.sharding import PartitionSpec as P

eps = 1e-06
lru_power = 8.0


def shifted(block, axis, distance):
    devices = range(lax.axis_size(axis))
    route = [(i - distance, i) for i in devices if i - distance in devices]
    return lax.ppermute(block, axis, route)


def sent_to_all(shard, axis):
    length = lax.axis_size(axis)
    return lax.all_to_all(
        jnp.broadcast_to(shard[None], (length, *shard.shape)), axis, 0, 0, tiled=True
    )


def collected_together(shard, axis):
    leaves = jax.tree.leaves(shard)
    turns = sorted(range(len(leaves)), key=lambda k: -leaves[k].size)
    width = (1, *leaves[turns[0]].shape)[-1]
    lines = [
        jnp.pad(leaves[k].reshape(-1), (0, -leaves[k].size % width)).reshape(-1, width)
        for k in turns
    ]
    both, at, found = (sent_to_all(jnp.concatenate(lines), axis), 0, {})
    for k, line in zip(turns, lines):
        share = both[:, at : at + len(line)].reshape(len(both), -1)
        found[k] = share[:, : leaves[k].size].reshape(-1, *leaves[k].shape)
        at += len(line)
    numbers = iter(range(len(leaves)))
    return jax.tree.map(lambda _: found[next(numbers)], shard)


def folded_in_pairs(pieces, combine):
    while len(jax.tree.leaves(pieces)[0]) > 1:
        pieces = jax.vmap(combine)(
            *(jax.tree.map(lambda part: part[side::2], pieces) for side in (0, 1))
        )
    return jax.tree.map(lambda part: part[0], pieces)


def carried_in(shard, axis, combine, identity):
    length, mine = (lax.axis_size(axis), lax.axis_index(axis))
    passed = jnp.arange(length) < mine

    def kept(part, zero, own):
        part = jnp.where(
            passed.reshape(-1, *(1 for _ in own.shape)), part, jnp.asarray(zero, own.dtype)
        )
        return part

    pieces = collected_together(shard, axis)
    return folded_in_pairs(jax.tree.map(kept, pieces, identity, shard), combine)


def sent_together(arrays, axis, dim, along):
    both = jnp.concatenate(arrays, axis=along)
    whole, at, outs = (lax.psum_scatter(both, axis, scatter_dimension=dim, tiled=True), 0, [])
    for a in arrays:
        outs.append(lax.slice_in_dim(whole, at, at + a.shape[along], axis=along))
        at += a.shape[along]
    return tuple(outs)


def rms_scale(values, scale):
    floats = values.astype(jnp.float32)
    return floats * lax.rsqrt(jnp.mean(floats * floats, axis=-1, keepdims=True) + eps) * scale


def linear_pair(earlier, later):
    return (earlier[0] * later[0], later[0] * earlier[1] + later[1])


def slot_table(route_ids, expert_count, capacity):
    id_list = route_ids.reshape(-1)
    indicator = (id_list[:, None] == jnp.arange(expert_count, dtype=jnp.int32)[None, :]).astype(
        jnp.int32
    )
    earlier_count = jnp.cumsum(indicator, axis=0) - indicator
    position = jnp.sum(earlier_count * indicator, axis=1)
    slot_ids = id_list * capacity + position
    matched = (
        slot_ids[None, :] == jnp.arange(expert_count * capacity, dtype=jnp.int32)[:, None]
    ).astype(jnp.int32)
    source = jnp.sum(matched * jnp.arange(id_list.shape[0], dtype=jnp.int32)[None, :], axis=1)
    filled = jnp.sum(matched, axis=1) > 0
    return (slot_ids, source, filled)


def body(
    mixer_rows,
    mixer_gain,
    gate_proj,
    input_proj,
    conv_taps,
    input_gates,
    decay_gates,
    decay_offset,
    out_proj,
    mixer_scale,
    expert_rows,
    expert_gain,
    route_ids,
    route_weights,
    expert_gate,
    expert_up,
    expert_down,
    shared_gate,
    shared_up,
    shared_down,
    expert_scale,
):
    row_count = mixer_rows.shape[0]
    normed = rms_scale(mixer_rows, mixer_gain).astype(jnp.bfloat16)
    gate_branch = jax.nn.gelu(jnp.dot(normed, gate_proj, preferred_element_type=jnp.float32))
    branch = jnp.dot(normed, input_proj, preferred_element_type=jnp.float32).astype(jnp.bfloat16)
    tap_count = conv_taps.shape[0]
    earlier_rows = shifted(branch[row_count - tap_count + 1 :], "ep", 1)
    padded = jnp.concatenate([earlier_rows, branch], axis=0)
    conv_sum = conv_taps[0] * padded[0:row_count].astype(jnp.float32)
    for tap_index in range(1, tap_count):
        conv_sum = conv_sum + conv_taps[tap_index] * padded[
            tap_index : tap_index + row_count
        ].astype(jnp.float32)
    conv_out = conv_sum.astype(jnp.bfloat16)
    block_rows = conv_out.reshape(row_count, input_gates.shape[0], input_gates.shape[1])
    input_gate = jax.nn.sigmoid(
        jnp.einsum("rbi,bij->rbj", block_rows, input_gates, preferred_element_type=jnp.float32)
    ).reshape(row_count, -1)
    decay_gate = jax.nn.sigmoid(
        jnp.einsum("rbi,bij->rbj", block_rows, decay_gates, preferred_element_type=jnp.float32)
    ).reshape(row_count, -1)
    log_decay = -lru_power * decay_gate * jax.nn.softplus(-decay_offset)
    positions = lax.axis_index("ep") * row_count + jnp.arange(row_count, dtype=jnp.int32)
    input_scale = jnp.where((positions == 0)[:, None], 1.0, jnp.sqrt(-jnp.expm1(2.0 * log_decay)))
    drive_term = input_scale * input_gate * conv_out.astype(jnp.float32)
    decay_rate = jnp.exp(log_decay)
    decay_product, local_states = lax.associative_scan(
        linear_pair, (decay_rate, drive_term), axis=0
    )
    carried = carried_in(
        (decay_product[-1], local_states[-1]),
        "ep",
        linear_pair,
        (jnp.ones_like(decay_rate[0]), jnp.zeros_like(decay_rate[0])),
    )
    states = local_states + decay_product * carried[1][None, :]
    gated_rows = (gate_branch * states).astype(jnp.bfloat16)
    mixer_term = jnp.dot(gated_rows, out_proj, preferred_element_type=jnp.float32)
    ep_size = lax.axis_size("ep")
    local_experts = expert_gate.shape[0]
    expert_count = local_experts * ep_size
    top_count = route_ids.shape[1]
    token_count = expert_rows.shape[0]
    row_width = expert_rows.shape[1]
    capacity = token_count * top_count * 3 // (2 * expert_count)
    expert_normed = rms_scale(expert_rows, expert_gain).astype(jnp.bfloat16)
    slot_ids, source, filled = slot_table(route_ids, expert_count, capacity)
    outgoing = jnp.where(
        filled[:, None], expert_normed[source // top_count], jnp.zeros((), jnp.bfloat16)
    )
    outgoing = outgoing.reshape(ep_size, local_experts, capacity, row_width)
    received = lax.all_to_all(outgoing, "ep", split_axis=0, concat_axis=0, tiled=True)
    gate_part = jnp.einsum(
        "secd,edf->secf", received, expert_gate, preferred_element_type=jnp.float32
    )
    up_part = jnp.einsum("secd,edf->secf", received, expert_up, preferred_element_type=jnp.float32)
    copy_hidden = (jax.nn.silu(gate_part) * up_part).astype(jnp.bfloat16)
    column_sums = lax.psum_scatter(
        jnp.einsum("secf,efd->secd", copy_hidden, expert_down, preferred_element_type=jnp.float32),
        "tp",
        scatter_dimension=3,
        tiled=True,
    )
    result = lax.all_to_all(column_sums, "ep", split_axis=0, concat_axis=0, tiled=True)
    flat_back = result.reshape(expert_count * capacity, -1)
    picked = flat_back[slot_ids] * route_weights.reshape(-1, 1)
    routed = jnp.sum(picked.reshape(token_count, top_count, -1), axis=1)
    shared_hidden = (
        jax.nn.silu(jnp.dot(expert_normed, shared_gate, preferred_element_type=jnp.float32))
        * jnp.dot(expert_normed, shared_up, preferred_element_type=jnp.float32)
    ).astype(jnp.bfloat16)
    shared_term = jnp.dot(shared_hidden, shared_down, preferred_element_type=jnp.float32)
    mixer_sum, expert_sum = sent_together((mixer_term, shared_term), "tp", 0, 1)
    expert_sum = expert_sum + lax.all_to_all(routed, "tp", split_axis=0, concat_axis=1, tiled=True)
    mixer_out = rms_scale(mixer_sum, mixer_scale).astype(jnp.bfloat16)
    expert_out = rms_scale(expert_sum, expert_scale).astype(jnp.bfloat16)
    return (mixer_out, expert_out)


def solution(mesh):
    placed = (
        P("ep", None),
        P(),
        P(None, "tp"),
        P(None, "tp"),
        P(None, "tp"),
        P("tp", None, None),
        P("tp", None, None),
        P("tp"),
        P("tp", None),
        P(),
        P("ep", None),
        P(),
        P("ep", None),
        P("ep", None),
        P("ep", None, "tp"),
        P("ep", None, "tp"),
        P("ep", "tp", None),
        P(None, "tp"),
        P(None, "tp"),
        P("tp", None),
        P(),
    )
    return jax.shard_map(
        body,
        mesh=mesh,
        in_specs=placed,
        out_specs=(P(("ep", "tp"), None), P(("ep", "tp"), None)),
        check_vma=False,
    )
```

profile of v0, /device:TPU:1, one launch (start us, length us, event | category | flops | bytes accessed | tf_op | source)
XLA Modules:
  0.0 264.7 jit_solution(15755040382263902929)
XLA Ops:
  8.4 2.1 fusion.7
  12.7 2.2 fusion.9
  14.9 5.7 %gather_fusion = bf16[768,4096]{1,0:T(8,128)(2,1)} fusion(bf16[256,4096]{1,0:T(8,128)(2,1)S(1)} %fusion.9, s32[1024]{0:T(1024)S(1)} %pad_clamp_fusion.1), kind=kCustom, calls=%fused_computation | custom fusion | bytes 12585984 | tf_op jit(solution)/shard_map/gather | solution.py:166
  20.6 3.3 %broadcast_select_fusion = bf16[16,1,48,4096]{3,2,1,0:T(8,128)(2,1)S(1)} fusion(bf16[16,1,48,4096]{3,2,1,0:T(8,128)(2,1)} %bitcast.125, pred[16,48]{1,0:T(8,128)(4,1)S(1)} %gt.11), kind=kLoop, calls=%fused_computation.8 | loop fusion | flops 3145728 | bytes 12583680 | tf_op jit(solution)/shard_map/jit(_where)/select_n | solution.py:165
  23.9 80.6 %all_to_all.34 = bf16[16,1,48,4096]{3,2,1,0:T(8,128)(2,1)S(1)} all-to-all(bf16[16,1,48,4096]{3,2,1,0:T(8,128)(2,1)S(1)} %broadcast_select_fusion), channel_id=1, replica_groups=mesh['ep'=16,'tp'=8] {'ep'}, dimensions={0} | all-to-all | bytes 12582912 | tf_op jit(solution)/shard_map/all_to_all | solution.py:169
  104.5 2.6 copy-done.2
  108.9 14.1 %convolution_bitcast_fusion = f32[16,1,48,4096]{3,2,0,1:T(8,128)} fusion(bf16[1,128,4096]{2,1,0:T(8,128)(2,1)S(1)} %copy-done, bf16[16,1,48,4096]{3,2,1,0:T(8,128)(2,1)} %copy-done.2, bf16[1,4096,128]{2,1,0:T(8,128)(2,1)} %param.36, f32[16,1,48,128]{3,2,0,1:T(8,128)S(1)} %fusion.16), kind=kOutput, calls=%fused_computation.3 | convolution fusion | flops 1611202560 | bytes 21364736 | tf_op jit(solution)/shard_map/secf,efd->secd/dot_general | solution.py:176
  123.1 2.1 fusion.4
  125.2 4.2 %convolution_convert_fusion = bf16[256,512]{1,0:T(8,128)(2,1)S(1)} fusion(bf16[4096,512]{1,0:T(8,128)(2,1)} %param.24, bf16[256,4096]{1,0:T(8,128)(2,1)} %param.21, f32[4096]{0:T(1024)S(1)} %copy-done.8, f32[256]{0:T(256)S(1)} %add_rsqrt_fusion.1), kind=kOutput, calls=%fused_computation.32 | convolution fusion | flops 1078067200 | bytes 6571008 | tf_op jit(solution)/shard_map/dot_general | solution.py:122
  130.0 2.8 %collective-permute-start = (bf16[3,512]{1,0:T(4,128)(2,1)}, bf16[3,512]{1,0:T(4,128)(2,1)}, u32[]{:S(2)}, u32[]{:S(2)}) collective-permute-start(bf16[3,512]{1,0:T(4,128)(2,1)} %slice.435), channel_id=1, source_target_pairs={{0,8},{8,16},{16,24},{24,32},{32,40},{40,48},{48,56},{56,64},{64,7... | collective-permute-start | bytes 9224 | tf_op jit(solution)/shard_map/ppermute | solution.py:13
  134.7 4.9 %fusion.32 = f32[256,4096]{1,0:T(8,128)} fusion(bf16[128,4096]{1,0:T(8,128)(2,1)} %param.40, bf16[256,4096]{1,0:T(8,128)(2,1)S(1)} %fusion.9, bf16[4096,128]{1,0:T(8,128)(2,1)} %param.39, f32[256,128]{1,0:T(8,128)S(1)} %fusion.117), kind=kOutput, calls=%fused_computation.38 | convolution fusion | flops 537067520 | bytes 8519680 | tf_op jit(solution)/shard_map/dot_general | solution.py:189
  151.3 2.0 fusion.74
  161.7 4.9 %all-to-all-start = ((f32[16,2,512]{2,1,0:T(2,128)}), f32[16,2,512]{2,1,0:T(2,128)S(1)}, u32[]{:S(2)}, u32[]{:S(2)}) async-start(f32[16,2,512]{2,1,0:T(2,128)} %broadcast_in_dim.44), calls=%async_computation | async-start | bytes 131072 | tf_op jit(solution)/shard_map/all_to_all | solution.py:18
  166.6 6.5 %all-to-all-done = f32[16,2,512]{2,1,0:T(2,128)S(1)} async-done(((f32[16,2,512]{2,1,0:T(2,128)}), f32[16,2,512]{2,1,0:T(2,128)S(1)}, u32[]{:S(2)}, u32[]{:S(2)}) %all-to-all-start) | async-done | bytes 65568 | tf_op jit(solution)/shard_map/all_to_all | solution.py:18
  173.5 8.6 %fusion.59 = f32[256,4096]{1,0:T(8,128)} fusion(bf16[512,4096]{1,0:T(8,128)(2,1)} %param.29, bf16[4096,512]{1,0:T(8,128)(2,1)} %param.23, bf16[256,4096]{1,0:T(8,128)(2,1)S(1)} %copy-done.3, f32[4096]{0:T(1024)S(1)} %copy-done.9, f32[256]{0:T(256)S(1)} %copy-done.15, f32[256,512]{1,0:T(8,128)S(1)} %pad.128, f32[256,512]{1,0:T(8,128)S(1)} %copy-done.4, ...), kind=kOutput, calls=%fused_computation.54 | convolution fusion | flops 2153512960 | bytes 16796672 | tf_op jit(solution)/shard_map/dot_general | solution.py:155
  182.1 7.7 %pad_maximum_fusion = f32[256,8192]{1,0:T(8,128)} fusion(f32[256,4096]{1,0:T(8,128)} %fusion.32, f32[256,4096]{1,0:T(8,128)} %fusion.59), kind=kLoop, calls=%fused_computation.2 | loop fusion | flops 2097152 | bytes 16777216 | tf_op jit(solution)/shard_map/concatenate | solution.py:63
  189.9 4.3 %reduce-scatter.5.cloned.1.call-done = f32[16,1,48,512]{3,2,0,1:T(8,128)} async-done(((f32[16,1,48,4096]{3,2,0,1:T(8,128)}), f32[16,1,48,512]{3,2,0,1:T(8,128)}) %reduce-scatter.5.cloned.1.call-update) | async-done | bytes 1572880 | tf_op jit(solution)/shard_map/reduce_scatter | solution.py:175
  194.1 6.7 %all-to-all-start.2 = ((f32[16,1,48,512]{3,2,1,0:T(8,128)}), f32[16,1,48,512]{3,2,1,0:T(8,128)S(1)}, u32[]{:S(2)}, u32[]{:S(2)}) async-start(f32[16,1,48,512]{3,2,1,0:T(8,128)} %bitcast.130), calls=%async_computation.4 | async-start | bytes 3145728 | tf_op jit(solution)/shard_map/all_to_all | solution.py:181
  201.3 20.8 %all-to-all-done.2 = f32[16,1,48,512]{3,2,1,0:T(8,128)S(1)} async-done(((f32[16,1,48,512]{3,2,1,0:T(8,128)}), f32[16,1,48,512]{3,2,1,0:T(8,128)S(1)}, u32[]{:S(2)}, u32[]{:S(2)}) %all-to-all-start.2) | async-done | bytes 1572896 | tf_op jit(solution)/shard_map/all_to_all | solution.py:181
  222.1 2.3 gather_fusion.1
  224.4 2.0 gather.13
  227.7 22.3 %all_to_all.35 = f32[8,32,512]{2,1,0:T(8,128)S(1)} all-to-all(f32[8,32,512]{2,1,0:T(8,128)S(1)} %bitcast.128), channel_id=1, replica_groups=mesh['ep'=16,'tp'=8] {'tp'}, dimensions={0} | all-to-all | bytes 1048576 | tf_op jit(solution)/shard_map/all_to_all | solution.py:191
  250.1 4.2 %reduce-scatter.3.cloned.1.call-done = f32[32,8192]{1,0:T(8,128)} async-done(((f32[256,8192]{1,0:T(8,128)}), f32[32,8192]{1,0:T(8,128)}) %reduce-scatter.3.cloned.1.call-update) | async-done | bytes 1048592 | tf_op jit(solution)/shard_map/reduce_scatter | solution.py:64
  255.7 2.2 multiply_convert_fusion
  (229 shorter events, 30.7 us)
Async XLA Ops:
  7.2 101.7 %copy-start = (bf16[1,128,4096]{2,1,0:T(8,128)(2,1)S(1)}, bf16[1,128,4096]{2,1,0:T(8,128)(2,1)}, u32[]{:S(2)}) copy-start(bf16[1,128,4096]{2,1,0:T(8,128)(2,1)} %param.37) | copy-start | bytes 3145732
  7.2 187.0 %reduce-scatter.5.cloned.1.call-start = ((), (), s32[]{:S(2)}) async-start(), calls=%async_computation.7 | async-start | bytes 14155776 | tf_op jit(solution)/shard_map/reduce_scatter | solution.py:175
  23.9 83.2 %copy-start.18 = (bf16[1,4096,128]{2,1,0:T(8,128)(2,1)S(1)}, bf16[1,4096,128]{2,1,0:T(8,128)(2,1)}, u32[]{:S(2)}) copy-start(bf16[1,4096,128]{2,1,0:T(8,128)(2,1)} %param.35) | copy-start | bytes 3145732
  104.5 2.6 copy-start.2
  125.2 4.3 %copy-start.14 = (f32[256]{0:T(256)}, f32[256]{0:T(256)S(1)}, u32[]{:S(2)}) copy-start(f32[256]{0:T(256)S(1)} %add_rsqrt_fusion.1) | copy-start | bytes 3076
  125.2 7.6 %copy-start.17 = (f32[512]{0:T(512)S(1)}, f32[512]{0:T(512)}, u32[]{:S(2)}) copy-start(f32[512]{0:T(512)} %param.28) | copy-start | bytes 6148
  125.2 8.2 %copy-start.12 = (f32[4,512]{1,0:T(4,128)S(1)}, f32[4,512]{1,0:T(4,128)}, u32[]{:S(2)}) copy-start(f32[4,512]{1,0:T(4,128)} %param.25) | copy-start | bytes 24580
  125.2 8.8 %copy-start.5 = (bf16[4096,128]{1,0:T(8,128)(2,1)S(1)}, bf16[4096,128]{1,0:T(8,128)(2,1)}, u32[]{:S(2)}) copy-start(bf16[4096,128]{1,0:T(8,128)(2,1)} %param.38) | copy-start | bytes 3145732
  130.0 9.6 %collective-permute-start = (bf16[3,512]{1,0:T(4,128)(2,1)}, bf16[3,512]{1,0:T(4,128)(2,1)}, u32[]{:S(2)}, u32[]{:S(2)}) collective-permute-start(bf16[3,512]{1,0:T(4,128)(2,1)} %slice.435), channel_id=1, source_target_pairs={{0,8},{8,16},{16,24},{24,32},{32,40},{40,48},{48,56},{56,64},{64,7... | collective-permute-start | bytes 9224 | tf_op jit(solution)/shard_map/ppermute | solution.py:13
  134.7 4.9 %copy-start.11 = (f32[1,512]{1,0:T(1,128)S(1)}, f32[1,512]{1,0:T(1,128)}, u32[]{:S(2)}) copy-start(f32[1,512]{1,0:T(1,128)} %get-tuple-element.47) | copy-start | bytes 6148
  134.7 6.0 %copy-start.19 = (bf16[2,256,256]{2,1,0:T(8,128)(2,1)S(1)}, bf16[2,256,256]{2,1,0:T(8,128)(2,1)}, u32[]{:S(2)}) copy-start(bf16[2,256,256]{2,1,0:T(8,128)(2,1)} %param.27) | copy-start | bytes 786436
  139.6 2.2 copy-start.13
  151.1 22.4 %copy-start.3 = (bf16[256,4096]{1,0:T(8,128)(2,1)S(1)}, bf16[256,4096]{1,0:T(8,128)(2,1)}, u32[]{:S(2)}) copy-start(bf16[256,4096]{1,0:T(8,128)(2,1)} %param.21) | copy-start | bytes 6291460
  151.1 22.4 %copy-start.9 = (f32[4096]{0:T(1024)S(1)}, f32[4096]{0:T(1024)}, u32[]{:S(2)}) copy-start(f32[4096]{0:T(1024)} %param.22) | copy-start | bytes 49156
  151.1 22.4 %copy-start.15 = (f32[256]{0:T(256)S(1)}, f32[256]{0:T(256)}, u32[]{:S(2)}) copy-start(f32[256]{0:T(256)} %copy-done.14) | copy-start | bytes 3076
  153.3 20.2 %copy-start.4 = (f32[256,512]{1,0:T(8,128)S(1)}, f32[256,512]{1,0:T(8,128)}, u32[]{:S(2)}) copy-start(f32[256,512]{1,0:T(8,128)} %pad.129) | copy-start | bytes 1572868
  161.7 11.4 %all-to-all-start = ((f32[16,2,512]{2,1,0:T(2,128)}), f32[16,2,512]{2,1,0:T(2,128)S(1)}, u32[]{:S(2)}, u32[]{:S(2)}) async-start(f32[16,2,512]{2,1,0:T(2,128)} %broadcast_in_dim.44), calls=%async_computation | async-start | bytes 131072 | tf_op jit(solution)/shard_map/all_to_all | solution.py:18
  166.5 87.7 %reduce-scatter.3.cloned.1.call-start = ((), (), s32[]{:S(2)}) async-start(), calls=%async_computation.6 | async-start | bytes 9437184 | tf_op jit(solution)/shard_map/reduce_scatter | solution.py:64
  189.8 11.0 %copy-start.10 = (s32[256,2]{0,1:T(2,128)S(1)}, s32[256,2]{0,1:T(2,128)}, u32[]{:S(2)}) copy-start(s32[256,2]{0,1:T(2,128)} %param.33) | copy-start | bytes 6148
  189.8 11.3 %copy-start.16 = (f32[256,2]{0,1:T(2,128)S(1)}, f32[256,2]{0,1:T(2,128)}, u32[]{:S(2)}) copy-start(f32[256,2]{0,1:T(2,128)} %param.34) | copy-start | bytes 6148
  194.1 27.9 %all-to-all-start.2 = ((f32[16,1,48,512]{3,2,1,0:T(8,128)}), f32[16,1,48,512]{3,2,1,0:T(8,128)S(1)}, u32[]{:S(2)}, u32[]{:S(2)}) async-start(f32[16,1,48,512]{3,2,1,0:T(8,128)} %bitcast.130), calls=%async_computation.4 | async-start | bytes 3145728 | tf_op jit(solution)/shard_map/all_to_all | solution.py:181
  224.4 31.3 %copy-start.6 = (f32[4096]{0:T(1024)S(1)}, f32[4096]{0:T(1024)}, u32[]{:S(2)}) copy-start(f32[4096]{0:T(1024)} %param.41) | copy-start | bytes 49156
  224.4 31.3 %copy-start.7 = (f32[4096]{0:T(1024)S(1)}, f32[4096]{0:T(1024)}, u32[]{:S(2)}) copy-start(f32[4096]{0:T(1024)} %param.30) | copy-start | bytes 49156
  224.4 33.5 %copy-start.1 = (bf16[1,128,4096]{2,1,0:T(8,128)(2,1)S(1)}, bf16[1,128,4096]{2,1,0:T(8,128)(2,1)}, u32[]{:S(2)}) copy-start(bf16[1,128,4096]{2,1,0:T(8,128)(2,1)} %param.37) | copy-start | bytes 3145732
  (2 other events, 3.8 us)
Sparse Core Ops, SparseCore 0:
  123.2 70.9 reduce-scatter.4
  196.5 57.6 reduce-scatter.2
where the time goes:
time: 265 us
  blocking collectives  103 us (39%)
  waiting for transfers between devices  35.7 us (13%)
  matrix products  35 us (13%)
  other arithmetic  32.2 us (12%)
  local copies, waits for them, and re-layouts  29.4 us (11%)
  between operations  15.1 us (6%)
  starting transfers between devices  14.4 us (5%)
    all_to_all x1, blocking collectives, body(): lax.all_to_all(outgoing, 'ep', split_axis=0, concat_axis=0, tiled=True)  80.6 us
    all_to_all x1, blocking collectives, body(): lax.all_to_all(routed, 'tp', split_axis=0, concat_axis=1, tiled=True)  22.3 us
    all_to_all x1, waiting for transfers between devices, body(): lax.all_to_all(column_sums, 'ep', split_axis=0, concat_axis=0, tiled=True)  20.8 us
    dot_general x1, matrix products, body(): jnp.einsum('secf,efd->secd', copy_hidden, expert_down, preferred_element_...  14.1 us
    dot_general x1, matrix products, body(): jnp.dot(gated_rows, out_proj, preferred_element_type=jnp.float32)  8.58 us
    concatenate x1, other arithmetic, sent_together(): both = jnp.concatenate(arrays, axis=along)  7.72 us
    all_to_all x1, starting transfers between devices, body(): lax.all_to_all(column_sums, 'ep', split_axis=0, concat_axis=0, tiled=True)  6.68 us
    pad x28, local copies, waits for them, and re-layouts, body(): lax.associative_scan(linear_pair, (decay_rate, drive_term), axis=0)  6.67 us
  transfers between devices with their start and end apart: 5, of which 4 were waited for; matrix products, arithmetic and copies ran while one was open for 22% of the time, Pallas kernels for 0%

commit v1 on v0

--- a/solution.py
+++ b/solution.py
@@ -2,9 +2,22 @@
 import jax.numpy as jnp
 from jax import lax
 from jax.sharding import PartitionSpec as P
+from jax.lax import axis_index, axis_size, ppermute
 
 eps = 1e-06
 lru_power = 8.0
+
+
+def cubes_update(arr, dim_i, array_in):
+    q_next = arr.shape
+    answer = arr.reshape(*q_next[:dim_i], array_in, q_next[dim_i] // array_in, *q_next[dim_i + 1 :])
+    return jnp.moveaxis(answer, dim_i, 0)
+
+
+def replace_the_links(xx, d0):
+    xx = jnp.moveaxis(xx, 0, d0)
+    y_new = xx.shape
+    return xx.reshape(*y_new[:d0], y_new[d0] * y_new[d0 + 1], *y_new[d0 + 2 :])
 
 
 def shifted(block, axis, distance):
@@ -178,7 +191,18 @@
         scatter_dimension=3,
         tiled=True,
     )
-    result = lax.all_to_all(column_sums, "ep", split_axis=0, concat_axis=0, tiled=True)
+    b_next, v_next = (axis_size("ep"), axis_index("ep"))
+    d_next = cubes_update(column_sums, 0, b_next)
+    arrivals = [d_next[v_next]]
+    for j in tuple(range(1, b_next)):
+        current_block = d_next[(v_next + j) % b_next]
+        arrivals.append(
+            ppermute(
+                current_block, axis_name="ep", perm=[(c, (c + j) % b_next) for c in range(b_next)]
+            )
+        )
+    d_next = jnp.stack(arrivals)[(v_next - jnp.arange(b_next)) % b_next]
+    result = replace_the_links(d_next, 0)
     flat_back = result.reshape(expert_count * capacity, -1)
     picked = flat_back[slot_ids] * route_weights.reshape(-1, 1)
     routed = jnp.sum(picked.reshape(token_count, top_count, -1), axis=1)

time: 265 us -> 268 us (1.011)
  starting transfers between devices: 14.4 us -> 36.3 us
  waiting for transfers between devices: 35.7 us -> 17.5 us
  blocking collectives: 103 us -> 99.7 us
  local copies, waits for them, and re-layouts: 29.4 us -> 32.6 us
    ppermute x0 -> x15, starting transfers between devices: none -> 28.5 us  [body(): ppermute(current_block, axis_name='ep', perm=[(c, (c + j) % b_next) for c...]
    all_to_all x1 -> x0, waiting for transfers between devices: 20.8 us -> none  [body(): lax.all_to_all(column_sums, 'ep', split_axis=0, concat_axis=0, tiled=True)]
    all_to_all x1 -> x0, starting transfers between devices: 6.68 us -> none  [body(): lax.all_to_all(column_sums, 'ep', split_axis=0, concat_axis=0, tiled=True)]
    reduce_scatter x1, waiting for transfers between devices: 4.21 us -> 0.02 us  [sent_together(): lax.psum_scatter(both, axis, scatter_dimension=dim, tiled=True)]
    ppermute x0 -> x15, waiting for transfers between devices: none -> 3.41 us  [body(): ppermute(current_block, axis_name='ep', perm=[(c, (c + j) % b_next) for c...]
    reduce_scatter x1, waiting for transfers between devices: 4.28 us -> 7.53 us  [body(): lax.psum_scatter(jnp.einsum('secf,efd->secd', copy_hidden, expert_down, p...]
    all_to_all x1, blocking collectives: 22.3 us -> 19.1 us  [body(): lax.all_to_all(routed, 'tp', split_axis=0, concat_axis=1, tiled=True)]
    unnamed x44 -> x71, local copies, waits for them, and re-layouts: 3.72 us -> 6.49 us
  transfers between devices with their start and end apart: 5 -> 19, of which waited for: 4 -> 6; matrix products, arithmetic and copies ran while one was open for 22% -> 21% of each run, Pallas kernels for 0% -> 0%
where the time goes in v1:
time: 268 us; the launch traced here: 267 us
  blocking collectives  99.7 us (37%)
  starting transfers between devices  36.3 us (14%)
  matrix products  34.4 us (13%)
  local copies, waits for them, and re-layouts  32.6 us (12%)
  other arithmetic  30.7 us (11%)
  waiting for transfers between devices  17.5 us (7%)
  between operations  15.7 us (6%)
    all_to_all x1, blocking collectives, body(): lax.all_to_all(outgoing, 'ep', split_axis=0, concat_axis=0, tiled=True)  80.6 us
    ppermute x15, starting transfers between devices, body(): ppermute(current_block, axis_name='ep', perm=[(c, (c + j) % b_next) for c...  28.5 us
    all_to_all x1, blocking collectives, body(): lax.all_to_all(routed, 'tp', split_axis=0, concat_axis=1, tiled=True)  19.1 us
    dot_general x1, matrix products, body(): jnp.einsum('secf,efd->secd', copy_hidden, expert_down, preferred_element_...  14.1 us
    dot_general x1, matrix products, body(): jnp.dot(gated_rows, out_proj, preferred_element_type=jnp.float32)  8.59 us
    concatenate x1, other arithmetic, sent_together(): both = jnp.concatenate(arrays, axis=along)  7.74 us
    reduce_scatter x1, waiting for transfers between devices, body(): lax.psum_scatter(jnp.einsum('secf,efd->secd', copy_hidden, expert_down, p...  7.53 us
    pad x28, local copies, waits for them, and re-layouts, body(): lax.associative_scan(linear_pair, (decay_rate, drive_term), axis=0)  6.69 us
  transfers between devices with their start and end apart: 19, of which 6 were waited for; matrix products, arithmetic and copies ran while one was open for 21% of the time, Pallas kernels for 0%

profile of v1, /device:TPU:1, one launch (start us, length us, event | category | flops | bytes accessed | tf_op | source)
XLA Modules:
  0.0 266.8 jit_solution(2413345070313781310)
XLA Ops:
  9.1 2.1 fusion.7
  13.7 2.2 fusion.9
  16.5 5.8 %gather_fusion = bf16[768,4096]{1,0:T(8,128)(2,1)} fusion(bf16[256,4096]{1,0:T(8,128)(2,1)S(1)} %fusion.9, s32[1024]{0:T(1024)S(1)} %get-tuple-element.71), kind=kCustom, calls=%fused_computation | custom fusion | bytes 12585984 | tf_op jit(solution)/shard_map/gather | solution.py:179
  22.3 3.3 %broadcast_select_fusion = bf16[16,1,48,4096]{3,2,1,0:T(8,128)(2,1)S(1)} fusion(bf16[16,1,48,4096]{3,2,1,0:T(8,128)(2,1)} %bitcast.173, pred[16,48]{1,0:T(8,128)(4,1)S(1)} %gt.11), kind=kLoop, calls=%fused_computation.9 | loop fusion | flops 3145728 | bytes 12583680 | tf_op jit(solution)/shard_map/jit(_where)/select_n | solution.py:178
  25.6 80.6 %all_to_all.29 = bf16[16,1,48,4096]{3,2,1,0:T(8,128)(2,1)S(1)} all-to-all(bf16[16,1,48,4096]{3,2,1,0:T(8,128)(2,1)S(1)} %broadcast_select_fusion), channel_id=1, replica_groups=mesh['ep'=16,'tp'=8] {'ep'}, dimensions={0} | all-to-all | bytes 12582912 | tf_op jit(solution)/shard_map/all_to_all | solution.py:182
  106.1 2.6 copy-done.2
  110.5 14.1 %convolution_bitcast_fusion = f32[16,1,48,4096]{3,2,0,1:T(8,128)} fusion(bf16[1,128,4096]{2,1,0:T(8,128)(2,1)S(1)} %copy-done, bf16[16,1,48,4096]{3,2,1,0:T(8,128)(2,1)} %copy-done.2, bf16[1,4096,128]{2,1,0:T(8,128)(2,1)} %param.36, f32[16,1,48,128]{3,2,0,1:T(8,128)S(1)} %fusion.16), kind=kOutput, calls=%fused_computation.4 | convolution fusion | flops 1611202560 | bytes 21364736 | tf_op jit(solution)/shard_map/secf,efd->secd/dot_general | solution.py:189
  124.7 2.2 fusion.4
  127.0 3.6 %convolution_convert_fusion = bf16[256,512]{1,0:T(8,128)(2,1)S(1)} fusion(bf16[4096,512]{1,0:T(8,128)(2,1)} %param.24, bf16[256,4096]{1,0:T(8,128)(2,1)S(1)} %copy-done.3, f32[4096]{0:T(1024)S(1)} %copy-done.12, f32[256]{0:T(256)S(1)} %add_rsqrt_fusion.1), kind=kOutput, calls=%fused_computation.33 | convolution fusion | flops 1078067200 | bytes 6571008 | tf_op jit(solution)/shard_map/dot_general | solution.py:135
  131.2 2.8 %collective-permute-start = (bf16[3,512]{1,0:T(4,128)(2,1)}, bf16[3,512]{1,0:T(4,128)(2,1)}, u32[]{:S(2)}, u32[]{:S(2)}) collective-permute-start(bf16[3,512]{1,0:T(4,128)(2,1)} %slice.437), channel_id=1, source_target_pairs={{0,8},{8,16},{16,24},{24,32},{32,40},{40,48},{48,56},{56,64},{64,7... | collective-permute-start | bytes 9224 | tf_op jit(solution)/shard_map/ppermute | solution.py:26
  135.9 4.9 %fusion.32 = f32[256,4096]{1,0:T(8,128)} fusion(bf16[128,4096]{1,0:T(8,128)(2,1)} %param.40, bf16[256,4096]{1,0:T(8,128)(2,1)S(1)} %fusion.9, bf16[4096,128]{1,0:T(8,128)(2,1)} %param.39, f32[256,128]{1,0:T(8,128)S(1)} %fusion.119), kind=kOutput, calls=%fused_computation.39 | convolution fusion | flops 537067520 | bytes 8519680 | tf_op jit(solution)/shard_map/dot_general | solution.py:213
  159.0 5.0 %all-to-all-start = ((f32[16,2,512]{2,1,0:T(2,128)}), f32[16,2,512]{2,1,0:T(2,128)S(1)}, u32[]{:S(2)}, u32[]{:S(2)}) async-start(f32[16,2,512]{2,1,0:T(2,128)} %broadcast_in_dim.44), calls=%async_computation | async-start | bytes 131072 | tf_op jit(solution)/shard_map/all_to_all | solution.py:31
  164.0 6.5 %all-to-all-done = f32[16,2,512]{2,1,0:T(2,128)S(1)} async-done(((f32[16,2,512]{2,1,0:T(2,128)}), f32[16,2,512]{2,1,0:T(2,128)S(1)}, u32[]{:S(2)}, u32[]{:S(2)}) %all-to-all-start) | async-done | bytes 65568 | tf_op jit(solution)/shard_map/all_to_all | solution.py:31
  170.9 8.6 %fusion.59 = f32[256,4096]{1,0:T(8,128)} fusion(bf16[512,4096]{1,0:T(8,128)(2,1)} %param.29, bf16[4096,512]{1,0:T(8,128)(2,1)} %param.23, bf16[256,4096]{1,0:T(8,128)(2,1)S(1)} %copy-done.4, f32[4096]{0:T(1024)S(1)} %copy-done.12, f32[256]{0:T(256)S(1)} %copy-done.21, f32[256,512]{1,0:T(8,128)S(1)} %pad.128, f32[256,512]{1,0:T(8,128)S(1)} %copy-done.6, ...), kind=kOutput, calls=%fused_computation.55 | convolution fusion | flops 2153512960 | bytes 16796672 | tf_op jit(solution)/shard_map/dot_general | solution.py:168
  179.5 7.7 %pad_maximum_fusion = f32[256,8192]{1,0:T(8,128)} fusion(f32[256,4096]{1,0:T(8,128)} %fusion.32, f32[256,4096]{1,0:T(8,128)} %fusion.59), kind=kLoop, calls=%fused_computation.3 | loop fusion | flops 2097152 | bytes 16777216 | tf_op jit(solution)/shard_map/concatenate | solution.py:76
  188.2 7.5 %reduce-scatter.5.cloned.1.call-done = f32[16,1,48,512]{3,2,0,1:T(8,128)} async-done(((f32[16,1,48,4096]{3,2,0,1:T(8,128)}), f32[16,1,48,512]{3,2,0,1:T(8,128)}) %reduce-scatter.5.cloned.1.call-update) | async-done | bytes 1572880 | tf_op jit(solution)/shard_map/reduce_scatter | solution.py:188
  198.5 2.4 collective-permute-start.2
  200.9 2.2 collective-permute-start.3
  208.6 3.2 %collective-permute-start.7 = (f32[1,1,48,512]{3,2,1,0:T(8,128)S(1)}, f32[1,1,48,512]{3,2,1,0:T(8,128)S(1)}, u32[]{:S(2)}, u32[]{:S(2)}) collective-permute-start(f32[1,1,48,512]{3,2,1,0:T(8,128)S(1)} %get-tuple-element.13), channel_id=1, source_target_pairs={{0,56},{8,64},{16,72},{24,80},{32,88},{40,96},{48,104},{56,112},{6... | collective-permute-start | bytes 294920 | tf_op jit(solution)/shard_map/ppermute | solution.py:200
  213.5 2.4 collective-permute-start.9
  215.9 2.6 collective-permute-start.10
  218.5 3.0 %collective-permute-start.11 = (f32[1,1,48,512]{3,2,1,0:T(8,128)S(1)}, f32[1,1,48,512]{3,2,1,0:T(8,128)S(1)}, u32[]{:S(2)}, u32[]{:S(2)}) collective-permute-start(f32[1,1,48,512]{3,2,1,0:T(8,128)S(1)} %get-tuple-element.9), channel_id=1, source_target_pairs={{0,88},{8,96},{16,104},{24,112},{32,120},{40,0},{48,8},{56,16},{64... | collective-permute-start | bytes 294920 | tf_op jit(solution)/shard_map/ppermute | solution.py:200
  221.5 2.1 collective-permute-start.12
  238.1 19.1 %all_to_all.30 = f32[8,32,512]{2,1,0:T(8,128)S(1)} all-to-all(f32[8,32,512]{2,1,0:T(8,128)S(1)} %bitcast.176), channel_id=1, replica_groups=mesh['ep'=16,'tp'=8] {'tp'}, dimensions={0} | all-to-all | bytes 1048576 | tf_op jit(solution)/shard_map/all_to_all | solution.py:215
  (289 shorter events, 54.7 us)
Async XLA Ops:
  7.2 103.3 %copy-start = (bf16[1,128,4096]{2,1,0:T(8,128)(2,1)S(1)}, bf16[1,128,4096]{2,1,0:T(8,128)(2,1)}, u32[]{:S(2)}) copy-start(bf16[1,128,4096]{2,1,0:T(8,128)(2,1)} %param.37) | copy-start | bytes 3145732
  7.2 188.6 %reduce-scatter.5.cloned.1.call-start = ((), (), s32[]{:S(2)}) async-start(), calls=%async_computation.6 | async-start | bytes 14155776 | tf_op jit(solution)/shard_map/reduce_scatter | solution.py:188
  25.5 83.2 %copy-start.24 = (bf16[1,4096,128]{2,1,0:T(8,128)(2,1)S(1)}, bf16[1,4096,128]{2,1,0:T(8,128)(2,1)}, u32[]{:S(2)}) copy-start(bf16[1,4096,128]{2,1,0:T(8,128)(2,1)} %param.35) | copy-start | bytes 3145732
  131.2 9.7 %collective-permute-start = (bf16[3,512]{1,0:T(4,128)(2,1)}, bf16[3,512]{1,0:T(4,128)(2,1)}, u32[]{:S(2)}, u32[]{:S(2)}) collective-permute-start(bf16[3,512]{1,0:T(4,128)(2,1)} %slice.437), channel_id=1, source_target_pairs={{0,8},{8,16},{16,24},{24,32},{32,40},{40,48},{48,56},{56,64},{64,7... | collective-permute-start | bytes 9224 | tf_op jit(solution)/shard_map/ppermute | solution.py:26
  151.3 19.6 %copy-start.21 = (f32[256]{0:T(256)S(1)}, f32[256]{0:T(256)}, u32[]{:S(2)}) copy-start(f32[256]{0:T(256)} %copy-done.20) | copy-start | bytes 3076
  159.0 11.5 %all-to-all-start = ((f32[16,2,512]{2,1,0:T(2,128)}), f32[16,2,512]{2,1,0:T(2,128)S(1)}, u32[]{:S(2)}, u32[]{:S(2)}) async-start(f32[16,2,512]{2,1,0:T(2,128)} %broadcast_in_dim.44), calls=%async_computation | async-start | bytes 131072 | tf_op jit(solution)/shard_map/all_to_all | solution.py:31
  164.0 93.4 %reduce-scatter.3.cloned.1.call-start = ((), (), s32[]{:S(2)}) async-start(), calls=%async_computation.5 | async-start | bytes 9437184 | tf_op jit(solution)/shard_map/reduce_scatter | solution.py:77
  197.3 9.9 %collective-permute-start.1 = (f32[1,1,48,512]{3,2,1,0:T(8,128)S(1)}, f32[1,1,48,512]{3,2,1,0:T(8,128)S(1)}, u32[]{:S(2)}, u32[]{:S(2)}) collective-permute-start(f32[1,1,48,512]{3,2,1,0:T(8,128)S(1)} %get-tuple-element.19), channel_id=1, source_target_pairs={{0,8},{8,16},{16,24},{24,32},{32,40},{40,48},{48,56},{56,64},{64,7... | collective-permute-start | bytes 294920 | tf_op jit(solution)/shard_map/ppermute | solution.py:200
  198.5 10.0 %collective-permute-start.2 = (f32[1,1,48,512]{3,2,1,0:T(8,128)S(1)}, f32[1,1,48,512]{3,2,1,0:T(8,128)S(1)}, u32[]{:S(2)}, u32[]{:S(2)}) collective-permute-start(f32[1,1,48,512]{3,2,1,0:T(8,128)S(1)} %get-tuple-element.18), channel_id=1, source_target_pairs={{0,16},{8,24},{16,32},{24,40},{32,48},{40,56},{48,64},{56,72},{64,... | collective-permute-start | bytes 294920 | tf_op jit(solution)/shard_map/ppermute | solution.py:200
  200.9 10.9 %collective-permute-start.3 = (f32[1,1,48,512]{3,2,1,0:T(8,128)S(1)}, f32[1,1,48,512]{3,2,1,0:T(8,128)S(1)}, u32[]{:S(2)}, u32[]{:S(2)}) collective-permute-start(f32[1,1,48,512]{3,2,1,0:T(8,128)S(1)} %get-tuple-element.17), channel_id=1, source_target_pairs={{0,24},{8,32},{16,40},{24,48},{32,56},{40,64},{48,72},{56,80},{64,... | collective-permute-start | bytes 294920 | tf_op jit(solution)/shard_map/ppermute | solution.py:200
  203.1 10.4 %collective-permute-start.4 = (f32[1,1,48,512]{3,2,1,0:T(8,128)S(1)}, f32[1,1,48,512]{3,2,1,0:T(8,128)S(1)}, u32[]{:S(2)}, u32[]{:S(2)}) collective-permute-start(f32[1,1,48,512]{3,2,1,0:T(8,128)S(1)} %get-tuple-element.16), channel_id=1, source_target_pairs={{0,32},{8,40},{16,48},{24,56},{32,64},{40,72},{48,80},{56,88},{64,... | collective-permute-start | bytes 294920 | tf_op jit(solution)/shard_map/ppermute | solution.py:200
  204.4 11.5 %collective-permute-start.5 = (f32[1,1,48,512]{3,2,1,0:T(8,128)S(1)}, f32[1,1,48,512]{3,2,1,0:T(8,128)S(1)}, u32[]{:S(2)}, u32[]{:S(2)}) collective-permute-start(f32[1,1,48,512]{3,2,1,0:T(8,128)S(1)} %get-tuple-element.15), channel_id=1, source_target_pairs={{0,40},{8,48},{16,56},{24,64},{32,72},{40,80},{48,88},{56,96},{64,... | collective-permute-start | bytes 294920 | tf_op jit(solution)/shard_map/ppermute | solution.py:200
  207.2 11.3 %collective-permute-start.6 = (f32[1,1,48,512]{3,2,1,0:T(8,128)S(1)}, f32[1,1,48,512]{3,2,1,0:T(8,128)S(1)}, u32[]{:S(2)}, u32[]{:S(2)}) collective-permute-start(f32[1,1,48,512]{3,2,1,0:T(8,128)S(1)} %get-tuple-element.14), channel_id=1, source_target_pairs={{0,48},{8,56},{16,64},{24,72},{32,80},{40,88},{48,96},{56,104},{64... | collective-permute-start | bytes 294920 | tf_op jit(solution)/shard_map/ppermute | solution.py:200
  208.6 13.0 %collective-permute-start.7 = (f32[1,1,48,512]{3,2,1,0:T(8,128)S(1)}, f32[1,1,48,512]{3,2,1,0:T(8,128)S(1)}, u32[]{:S(2)}, u32[]{:S(2)}) collective-permute-start(f32[1,1,48,512]{3,2,1,0:T(8,128)S(1)} %get-tuple-element.13), channel_id=1, source_target_pairs={{0,56},{8,64},{16,72},{24,80},{32,88},{40,96},{48,104},{56,112},{6... | collective-permute-start | bytes 294920 | tf_op jit(solution)/shard_map/ppermute | solution.py:200
  211.8 11.8 %collective-permute-start.8 = (f32[1,1,48,512]{3,2,1,0:T(8,128)S(1)}, f32[1,1,48,512]{3,2,1,0:T(8,128)S(1)}, u32[]{:S(2)}, u32[]{:S(2)}) collective-permute-start(f32[1,1,48,512]{3,2,1,0:T(8,128)S(1)} %get-tuple-element.12), channel_id=1, source_target_pairs={{0,64},{8,72},{16,80},{24,88},{32,96},{40,104},{48,112},{56,120},{... | collective-permute-start | bytes 294920 | tf_op jit(solution)/shard_map/ppermute | solution.py:200
  213.5 11.5 %collective-permute-start.9 = (f32[1,1,48,512]{3,2,1,0:T(8,128)S(1)}, f32[1,1,48,512]{3,2,1,0:T(8,128)S(1)}, u32[]{:S(2)}, u32[]{:S(2)}) collective-permute-start(f32[1,1,48,512]{3,2,1,0:T(8,128)S(1)} %get-tuple-element.11), channel_id=1, source_target_pairs={{0,72},{8,80},{16,88},{24,96},{32,104},{40,112},{48,120},{56,0},{6... | collective-permute-start | bytes 294920 | tf_op jit(solution)/shard_map/ppermute | solution.py:200
  215.9 10.8 %collective-permute-start.10 = (f32[1,1,48,512]{3,2,1,0:T(8,128)S(1)}, f32[1,1,48,512]{3,2,1,0:T(8,128)S(1)}, u32[]{:S(2)}, u32[]{:S(2)}) collective-permute-start(f32[1,1,48,512]{3,2,1,0:T(8,128)S(1)} %get-tuple-element.10), channel_id=1, source_target_pairs={{0,80},{8,88},{16,96},{24,104},{32,112},{40,120},{48,0},{56,8},{64... | collective-permute-start | bytes 294920 | tf_op jit(solution)/shard_map/ppermute | solution.py:200
  218.5 9.3 %collective-permute-start.11 = (f32[1,1,48,512]{3,2,1,0:T(8,128)S(1)}, f32[1,1,48,512]{3,2,1,0:T(8,128)S(1)}, u32[]{:S(2)}, u32[]{:S(2)}) collective-permute-start(f32[1,1,48,512]{3,2,1,0:T(8,128)S(1)} %get-tuple-element.9), channel_id=1, source_target_pairs={{0,88},{8,96},{16,104},{24,112},{32,120},{40,0},{48,8},{56,16},{64... | collective-permute-start | bytes 294920 | tf_op jit(solution)/shard_map/ppermute | solution.py:200
  221.5 6.7 %collective-permute-start.12 = (f32[1,1,48,512]{3,2,1,0:T(8,128)S(1)}, f32[1,1,48,512]{3,2,1,0:T(8,128)S(1)}, u32[]{:S(2)}, u32[]{:S(2)}) collective-permute-start(f32[1,1,48,512]{3,2,1,0:T(8,128)S(1)} %get-tuple-element.8), channel_id=1, source_target_pairs={{0,96},{8,104},{16,112},{24,120},{32,0},{40,8},{48,16},{56,24},{64... | collective-permute-start | bytes 294920 | tf_op jit(solution)/shard_map/ppermute | solution.py:200
  223.6 5.1 %collective-permute-start.13 = (f32[1,1,48,512]{3,2,1,0:T(8,128)S(1)}, f32[1,1,48,512]{3,2,1,0:T(8,128)S(1)}, u32[]{:S(2)}, u32[]{:S(2)}) collective-permute-start(f32[1,1,48,512]{3,2,1,0:T(8,128)S(1)} %get-tuple-element.7), channel_id=1, source_target_pairs={{0,104},{8,112},{16,120},{24,0},{32,8},{40,16},{48,24},{56,32},{64... | collective-permute-start | bytes 294920 | tf_op jit(solution)/shard_map/ppermute | solution.py:200
  225.0 5.0 %collective-permute-start.14 = (f32[1,1,48,512]{3,2,1,0:T(8,128)S(1)}, f32[1,1,48,512]{3,2,1,0:T(8,128)S(1)}, u32[]{:S(2)}, u32[]{:S(2)}) collective-permute-start(f32[1,1,48,512]{3,2,1,0:T(8,128)S(1)} %get-tuple-element.6), channel_id=1, source_target_pairs={{0,112},{8,120},{16,0},{24,8},{32,16},{40,24},{48,32},{56,40},{64,... | collective-permute-start | bytes 294920 | tf_op jit(solution)/shard_map/ppermute | solution.py:200
  226.7 4.6 %collective-permute-start.15 = (f32[1,1,48,512]{3,2,0,1:T(8,128)S(1)}, f32[1,1,48,512]{3,2,0,1:T(8,128)S(1)}, u32[]{:S(2)}, u32[]{:S(2)}) collective-permute-start(f32[1,1,48,512]{3,2,0,1:T(8,128)S(1)} %constant_dynamic-slice_fusion), channel_id=1, source_target_pairs={{0,120},{8,0},{16,8},{24,16},{32,24},{40,32},{48,40},{56,48},{64,5... | collective-permute-start | bytes 294920 | tf_op jit(solution)/shard_map/ppermute | solution.py:200
  238.1 20.8 %copy-start.10 = (f32[4096]{0:T(1024)S(1)}, f32[4096]{0:T(1024)}, u32[]{:S(2)}) copy-start(f32[4096]{0:T(1024)} %param.41) | copy-start | bytes 49156
  238.1 20.8 %copy-start.11 = (f32[4096]{0:T(1024)S(1)}, f32[4096]{0:T(1024)}, u32[]{:S(2)}) copy-start(f32[4096]{0:T(1024)} %param.30) | copy-start | bytes 49156
  (22 other events, 107.0 us)
Sparse Core Ops, SparseCore 0:
  124.8 70.9 reduce-scatter.4
  198.1 52.0 reduce-scatter.2
